TPU v7x, 32 devices: a whole 2x2x4 slice. The times are simulated.
32 devices in a mesh: sp: 4 (over y, x), dp: 8 (over z, core).
Axes of the slice: x: 2, y: 2, z: 4, core: 2. Of those that a mesh axis runs over, the one named last changes fastest.
Arguments:
- tokens: bfloat16 [8, 640, 2048], P('dp', 'sp'), may hold values from -42 to 42
- query_weight: bfloat16 [2048, 1024], P('dp'), may hold values from -1 to 1
- key_weight: bfloat16 [2048, 1024], P('dp'), may hold values from -1 to 1
- values: bfloat16 [8, 640, 1024], P('dp', 'sp'), may hold values from -6 to 6
- lambdas: float32 [16], replicated, may hold values from 0.3 to 0.8
- out_grad: bfloat16 [8, 640, 1024], P('dp', 'sp'), may hold values from -6 to 6
Outputs:
- tokens_grad: bfloat16 [8, 640, 2048], P('dp', 'sp')
- values_grad: bfloat16 [8, 640, 1024], P('dp', 'sp')
- query_weight_grad: float32 [2048, 1024], P('dp')
- key_weight_grad: float32 [2048, 1024], P('dp')
All inputs are finite; a program needn't handle non-finite values.
Results may differ from a plain program's by a relative error of at most 0.029.
The roundings to bfloat16 on the way count: a program that leaves them out, or rounds other values in their place, can miss the bound.
Values may be sent and summed in bfloat16 or wider, within the bound.
A program may use at most 128 MiB of HBM per device.

v0:
```python
import math

import jax
import jax.numpy as jnp
from jax import lax
from jax.sharding import PartitionSpec as P

DQK = 32


NORM_EPS = 0.1
THETA = 10000.0


def rotation_tables(positions, vec_width):
    half_width = vec_width // 2
    freqs = jnp.exp(-math.log(THETA) * jnp.arange(half_width, dtype=jnp.float32) / half_width)
    angles = positions.astype(jnp.float32)[:, None] * freqs[None, :]
    return (jnp.cos(angles), jnp.sin(angles))


def rotate(field, cosine, sine_table, vec_width, sign_value):
    full_shape = field.shape
    grouped = field.reshape(full_shape[:-1] + (full_shape[-1] // vec_width, 2, vec_width // 2))
    first_half = grouped[..., 0, :]
    second_half = grouped[..., 1, :]
    cos_cols = cosine[:, None, :]
    sin_cols = sign_value * sine_table[:, None, :]
    turned = jnp.stack(
        [
            first_half * cos_cols - second_half * sin_cols,
            second_half * cos_cols + first_half * sin_cols,
        ],
        axis=-2,
    )
    return turned.reshape(full_shape)


def pair_product(pattern, first_op, second_op):
    return jnp.einsum(pattern, first_op, second_op, preferred_element_type=jnp.float32)


def head_backward(query_rot, key_rot, value_rows, grad_rows, lambda_here, cosine, sine_table):
    seq_length = query_rot.shape[0]
    head_count = lambda_here.shape[0]
    qk_width = query_rot.shape[1] // (2 * head_count)
    value_width = value_rows.shape[1] // head_count
    block_rows = math.gcd(seq_length, 512)
    block_count = seq_length // block_rows
    inv_root = 1.0 / math.sqrt(qk_width)
    query_split = query_rot.reshape(block_count, block_rows, head_count, 2, qk_width)
    key_split = key_rot.reshape(seq_length, head_count, 2, qk_width)
    value_split = value_rows.reshape(seq_length, head_count, value_width)
    grad_split = grad_rows.reshape(block_count, block_rows, head_count, value_width)
    lambda_col = lambda_here[:, None, None]
    key_positions = jnp.arange(seq_length, dtype=jnp.int32)

    def block_step(carried, inputs):
        key_sum, value_sum = carried
        query_part, grad_part, block_start = inputs
        scores = pair_product("qhmd,khmd->hmqk", query_part, key_split) * inv_root
        query_positions = block_start + jnp.arange(block_rows, dtype=jnp.int32)
        causal_mask = key_positions[None, :] <= query_positions[:, None]
        scores = jnp.where(causal_mask, scores, -jnp.inf)
        row_max = jnp.max(scores, axis=-1, keepdims=True)
        exp_scores = jnp.exp(scores - row_max)
        prob_maps = exp_scores / jnp.sum(exp_scores, axis=-1, keepdims=True)
        weights = (prob_maps[:, 0] - lambda_col * prob_maps[:, 1]).astype(jnp.bfloat16)
        mixed_out = pair_product("hqk,khe->qhe", weights, value_split)
        norm_scale = lax.rsqrt(jnp.mean(mixed_out * mixed_out, axis=-1, keepdims=True) + NORM_EPS)
        grad_float = grad_part.astype(jnp.float32)
        mixed_grad = (
            norm_scale * grad_float
            - norm_scale
            * norm_scale
            * norm_scale
            * mixed_out
            * jnp.mean(grad_float * mixed_out, axis=-1, keepdims=True)
        ).astype(jnp.bfloat16)
        weight_grad = pair_product("qhe,khe->hqk", mixed_grad, value_split)
        value_sum = value_sum + pair_product("hqk,qhe->khe", weights, mixed_grad)
        first_grad = prob_maps[:, 0] * (
            weight_grad - jnp.sum(weight_grad * prob_maps[:, 0], axis=-1, keepdims=True)
        )
        second_grad = (
            -lambda_col
            * prob_maps[:, 1]
            * (weight_grad - jnp.sum(weight_grad * prob_maps[:, 1], axis=-1, keepdims=True))
        )
        score_grad = (jnp.stack([first_grad, second_grad], axis=1) * inv_root).astype(jnp.bfloat16)
        query_grad = pair_product("hmqk,khmd->qhmd", score_grad, key_split)
        key_sum = key_sum + pair_product("hmqk,qhmd->khmd", score_grad, query_part)
        return ((key_sum, value_sum), query_grad)

    zero_init = (
        jnp.zeros((seq_length, head_count, 2, qk_width), jnp.float32),
        jnp.zeros((seq_length, head_count, value_width), jnp.float32),
    )
    block_starts = jnp.arange(block_count, dtype=jnp.int32) * block_rows
    (key_sum, value_sum), query_blocks = lax.scan(
        block_step, zero_init, (query_split, grad_split, block_starts)
    )
    query_turned = query_blocks.reshape(seq_length, head_count * 2 * qk_width)
    key_turned = key_sum.reshape(seq_length, head_count * 2 * qk_width)
    query_back = rotate(query_turned, cosine, sine_table, qk_width, -1.0).astype(jnp.bfloat16)
    key_back = rotate(key_turned, cosine, sine_table, qk_width, -1.0).astype(jnp.bfloat16)
    values_back = value_sum.reshape(seq_length, head_count * value_width).astype(jnp.bfloat16)
    return (query_back, key_back, values_back)


def body(tokens, query_weight, key_weight, values, lambdas, out_grad):
    sp_count = lax.axis_size("sp")
    dp_count = lax.axis_size("dp")
    tok_rows = tokens.shape[1]
    head_total = lambdas.shape[0]
    token_block = tokens[0]
    positions = lax.axis_index("sp") * tok_rows + jnp.arange(tok_rows, dtype=jnp.int32)
    cosine, sine_table = rotation_tables(positions, DQK)
    whole_query, whole_key = (
        lax.all_gather(query_weight, "dp", axis=0, tiled=True),
        lax.all_gather(key_weight, "dp", axis=0, tiled=True),
    )
    query_raw = jnp.dot(token_block, whole_query, preferred_element_type=jnp.float32)
    key_raw = jnp.dot(token_block, whole_key, preferred_element_type=jnp.float32)
    query_rot = rotate(query_raw, cosine, sine_table, DQK, 1.0).reshape(
        tok_rows, head_total, 2 * DQK
    )
    key_rot = rotate(key_raw, cosine, sine_table, DQK, 1.0).reshape(tok_rows, head_total, 2 * DQK)
    packed = (
        jnp.stack((query_rot, key_rot), axis=2)
        .reshape(1, tok_rows, head_total * 4 * DQK)
        .astype(jnp.bfloat16)
    )
    packed_heads, values_heads, grad_heads = (
        lax.all_to_all(packed, "sp", split_axis=2, concat_axis=1, tiled=True),
        lax.all_to_all(values, "sp", split_axis=2, concat_axis=1, tiled=True),
        lax.all_to_all(out_grad, "sp", split_axis=2, concat_axis=1, tiled=True),
    )
    heads_here = head_total // sp_count
    lambda_here = lax.dynamic_slice_in_dim(lambdas, lax.axis_index("sp") * heads_here, heads_here)
    seq_length = tok_rows * sp_count
    cosine_all, sine_all = rotation_tables(jnp.arange(seq_length, dtype=jnp.int32), DQK)
    head_split = packed_heads[0].reshape(seq_length, heads_here, 2, 2 * DQK)
    query_heads = head_split[:, :, 0].reshape(seq_length, heads_here * 2 * DQK)
    key_heads = head_split[:, :, 1].reshape(seq_length, heads_here * 2 * DQK)
    query_back, key_back, values_back = head_backward(
        query_heads, key_heads, values_heads[0], grad_heads[0], lambda_here, cosine_all, sine_all
    )
    packed_back = jnp.stack(
        (
            query_back.reshape(seq_length, heads_here, 2 * DQK),
            key_back.reshape(seq_length, heads_here, 2 * DQK),
        ),
        axis=2,
    )
    packed_back = packed_back.reshape(1, seq_length, heads_here * 4 * DQK)
    packed_tokens, values_grad = (
        lax.all_to_all(packed_back, "sp", split_axis=1, concat_axis=2, tiled=True),
        lax.all_to_all(values_back[None], "sp", split_axis=1, concat_axis=2, tiled=True),
    )
    packed_rows = packed_tokens[0]
    back_split = packed_rows.reshape(tok_rows, head_total, 2, 2 * DQK)
    query_tok = back_split[:, :, 0].reshape(tok_rows, head_total * 2 * DQK)
    key_tok = back_split[:, :, 1].reshape(tok_rows, head_total * 2 * DQK)
    contract = (((1,), (1,)), ((), ()))
    tokens_grad = lax.dot_general(
        query_tok, whole_query, contract, preferred_element_type=jnp.float32
    ) + lax.dot_general(key_tok, whole_key, contract, preferred_element_type=jnp.float32)
    outer_rows = (((0,), (0,)), ((), ()))
    grad_shard = lax.psum_scatter(
        lax.dot_general(
            token_block, packed_rows, outer_rows, preferred_element_type=jnp.float32
        ).astype(jnp.bfloat16),
        "dp",
        scatter_dimension=0,
        tiled=True,
    )
    grad_total = lax.psum(grad_shard, "sp").astype(jnp.float32)
    factor = 1.0 / math.sqrt(dp_count * seq_length)
    total_split = grad_total.reshape(grad_total.shape[0], head_total, 2, 2 * DQK)
    query_weight_grad = (
        total_split[:, :, 0].reshape(grad_total.shape[0], head_total * 2 * DQK) * factor
    )
    key_weight_grad = (
        total_split[:, :, 1].reshape(grad_total.shape[0], head_total * 2 * DQK) * factor
    )
    return (tokens_grad.astype(jnp.bfloat16)[None], values_grad, query_weight_grad, key_weight_grad)


def solution(mesh):
    in_specs = (
        P("dp", "sp", None),
        P("dp", None),
        P("dp", None),
        P("dp", "sp", None),
        P(),
        P("dp", "sp", None),
    )
    out_specs = (P("dp", "sp", None), P("dp", "sp", None), P("dp", None), P("dp", None))
    return jax.shard_map(body, mesh=mesh, in_specs=in_specs, out_specs=out_specs, check_vma=False)
```

profile of v0, /device:TPU:0, one launch (start us, length us, event | category | flops | bytes accessed | tf_op | source)
XLA Modules:
  0.0 481.4 jit_solution(5948672629820562587)
XLA Ops:
  11.9 4.1 reduce.1
  17.4 5.4 %all-to-all-start.1 = ((bf16[4,2,20480]{2,1,0:T(2,128)(2,1)}), bf16[4,2,20480]{2,1,0:T(2,128)(2,1)S(1)}, u32[]{:S(2)}, u32[]{:S(2)}) async-start(bf16[4,2,20480]{2,1,0:T(2,128)(2,1)} %reshape.233), calls=%async_computation.1 | async-start | bytes 655360 | tf_op jit(solution)/shard_map/all_to_all | solution.py:136
  23.7 4.0 reduce.2
  29.4 31.4 %all-gather.5.cloned.1.call-done = bf16[2048,1024]{0,1:T(8,128)(2,1)} async-done(((bf16[256,1024]{0,1:T(8,128)(2,1)}), bf16[2048,1024]{0,1:T(8,128)(2,1)}) %all-gather.5.cloned.1.call-update) | async-done | bytes 4194320 | tf_op jit(solution)/shard_map/all_gather | solution.py:121
  60.7 5.0 %fusion.49 = f32[160,32,2,16]{0,1,3,2:T(8,128)S(1)} fusion(bf16[32,2,16,2048]{3,2,1,0:T(8,128)(2,1)} %bitcast.235, bf16[1,160,2048]{2,1,0:T(8,128)(2,1)S(1)} %copy-done), kind=kOutput, calls=%fused_computation.61 | convolution fusion | flops 671088640 | bytes 5505024 | tf_op jit(solution)/shard_map/dot_general | solution.py:124
  65.8 43.2 %all-gather.3.cloned.1.call-done = bf16[2048,1024]{0,1:T(8,128)(2,1)} async-done(((bf16[256,1024]{0,1:T(8,128)(2,1)}), bf16[2048,1024]{0,1:T(8,128)(2,1)}) %all-gather.3.cloned.1.call-update) | async-done | bytes 4194320 | tf_op jit(solution)/shard_map/all_gather | solution.py:120
  108.9 5.0 %fusion.51 = f32[160,32,2,16]{0,1,3,2:T(8,128)S(1)} fusion(bf16[32,2,16,2048]{3,2,1,0:T(8,128)(2,1)} %bitcast.236, bf16[1,160,2048]{2,1,0:T(8,128)(2,1)S(1)} %copy-done), kind=kOutput, calls=%fused_computation.63 | convolution fusion | flops 671088640 | bytes 5505024 | tf_op jit(solution)/shard_map/dot_general | solution.py:123
  115.0 3.9 all-to-all-start.2
  121.0 11.7 %copy.159 = bf16[1,160,2048]{1,0,2:T(2,128)(2,1)S(1)} copy(bf16[1,160,2048]{1,2,0:T(8,128)(2,1)S(1)} %bitcast.234) | data formatting | bytes 1310720 | tf_op jit(solution)/shard_map/convert_element_type | solution.py:132
  132.8 12.6 %reduce = bf16[2048,160]{1,0:T(8,128)(2,1)} reduce(bf16[2048,1,160]{2,1,0:T(2,128)(2,1)S(1)} %bitcast.228, bf16[]{:T(256)} %broadcast.188), dimensions={1}, to_apply=%bitcast.164.reduce_sub_computation | reduce | bytes 1310722
  145.3 3.4 reshape.231
  149.5 4.2 all-to-all-start
  169.3 130.5 %while.16 = (s32[]{:T(128)}, f32[640,4,2,32]{0,3,2,1:T(8,128)}, f32[640,4,64]{0,2,1:T(8,128)}, f32[5,128,4,2,32]{1,0,4,3,2:T(8,128)}, bf16[5,128,4,2,32]{1,4,3,2...) while((s32[]{:T(128)}, f32[640,4,2,32]{0,3,2,1:T(8,128)}, ...), condition=%wide.region_7.8_spmd.clone, body=%wide.region_0.7_spmd.clone.sunk | while | flops 389075456 | bytes 51640196 | solution.py:100
  170.8 3.4 fusion.143
  180.4 2.7 fusion.146
  183.1 2.7 fusion.145
  185.8 2.4 fusion.149
  189.9 4.7 dynamic_update_slice.7
  196.0 3.4 fusion.143
  206.7 2.7 fusion.146
  209.4 2.7 fusion.145
  212.2 2.4 fusion.149
  216.2 4.7 dynamic_update_slice.7
  222.3 3.4 fusion.143
  233.0 2.7 fusion.146
  235.7 2.7 fusion.145
  238.5 2.4 fusion.149
  242.6 4.7 dynamic_update_slice.7
  248.7 3.4 fusion.143
  257.2 2.2 fusion.148
  259.4 2.7 fusion.146
  262.1 2.7 fusion.145
  264.8 2.4 fusion.149
  268.9 4.7 dynamic_update_slice.7
  275.0 3.4 fusion.143
  285.7 2.7 fusion.146
  288.4 2.7 fusion.145
  291.1 2.4 fusion.149
  295.2 4.7 dynamic_update_slice.7
  303.8 4.6 reduce.3
  308.9 11.9 %all_to_all.78 = bf16[4,2,40960]{2,1,0:T(2,128)(2,1)S(1)} all-to-all(bf16[4,2,40960]{2,1,0:T(2,128)(2,1)S(1)} %reshape.237), channel_id=1, replica_groups=mesh['sp'=4,'dp'=8] {'sp'}, dimensions={0} | all-to-all | bytes 1310720 | tf_op jit(solution)/shard_map/all_to_all | solution.py:158
  322.3 5.6 %convert_bitcast_fusion = bf16[2048,2048]{0,1:T(8,128)(2,1)} fusion(bf16[160,2048]{1,0:T(8,128)(2,1)S(1)} %bitcast.244, bf16[1,160,2048]{2,1,0:T(8,128)(2,1)S(1)} %copy-done), kind=kOutput, calls=%fused_computation.60 | convolution fusion | flops 1346371584 | bytes 9699328 | tf_op jit(solution)/shard_map/dot_general | solution.py:171
  329.9 2.6 reduce.4
  333.3 3.5 all-to-all-start.4
  336.8 79.1 %reduce-scatter.2.cloned.1.call-done = bf16[256,2048]{0,1:T(8,128)(2,1)} async-done(((bf16[2048,2048]{0,1:T(8,128)(2,1)}), bf16[256,2048]{0,1:T(8,128)(2,1)}) %reduce-scatter.2.cloned.1.call-update) | async-done | bytes 1048592 | tf_op jit(solution)/shard_map/reduce_scatter | solution.py:170
  415.9 2.3 copy.137
  420.2 3.2 fusion.64
  425.7 44.7 %all-reduce.2.cloned.1.call-done = bf16[256,16,2,64]{0,3,1,2:T(8,128)(2,1)} async-done(((bf16[256,16,2,64]{0,3,1,2:T(8,128)(2,1)}), bf16[256,16,2,64]{0,3,1,2:T(8,128)(2,1)}) %all-reduce.2.cloned.1.call-update) | async-done | bytes 1048592 | tf_op jit(solution)/shard_map/psum | solution.py:178
  (219 shorter events, 93.2 us)
Async XLA Ops:
  7.2 53.6 %copy-start = (bf16[1,160,2048]{2,1,0:T(8,128)(2,1)S(1)}, bf16[1,160,2048]{2,1,0:T(8,128)(2,1)}, u32[]{:S(2)}) copy-start(bf16[1,160,2048]{2,1,0:T(8,128)(2,1)} %param.8) | copy-start | bytes 1966084
  7.2 2.3 copy-start.12
  7.2 53.5 %all-gather.5.cloned.1.call-start = ((), (), s32[]{:S(2)}) async-start(), calls=%async_computation.7 | async-start | bytes 4718592 | tf_op jit(solution)/shard_map/all_gather | solution.py:121
  9.4 1.1 copy-start.15
  9.4 99.5 %all-gather.3.cloned.1.call-start = ((), (), s32[]{:S(2)}) async-start(), calls=%async_computation.6 | async-start | bytes 4718592 | tf_op jit(solution)/shard_map/all_gather | solution.py:120
  11.9 11.0 %copy-start.16 = (bf16[1,160,1024]{2,1,0:T(8,128)(2,1)S(1)}, bf16[1,160,1024]{2,1,0:T(8,128)(2,1)}, u32[]{:S(2)}) copy-start(bf16[1,160,1024]{2,1,0:T(8,128)(2,1)} %param.13) | copy-start | bytes 983044
  17.4 97.6 %all-to-all-start.1 = ((bf16[4,2,20480]{2,1,0:T(2,128)(2,1)}), bf16[4,2,20480]{2,1,0:T(2,128)(2,1)S(1)}, u32[]{:S(2)}, u32[]{:S(2)}) async-start(bf16[4,2,20480]{2,1,0:T(2,128)(2,1)} %reshape.233), calls=%async_computation.1 | async-start | bytes 655360 | tf_op jit(solution)/shard_map/all_to_all | solution.py:136
  115.0 5.0 %copy-start.8 = (bf16[4,2,20480]{2,1,0:T(2,128)(2,1)}, bf16[4,2,20480]{2,1,0:T(2,128)(2,1)S(1)}, u32[]{:S(2)}) copy-start(bf16[4,2,20480]{2,1,0:T(2,128)(2,1)S(1)} %all-to-all-done.1) | copy-start | bytes 983044
  115.0 33.7 %all-to-all-start.2 = ((bf16[4,2,20480]{2,1,0:T(2,128)(2,1)}), bf16[4,2,20480]{2,1,0:T(2,128)(2,1)S(1)}, u32[]{:S(2)}, u32[]{:S(2)}) async-start(bf16[4,2,20480]{2,1,0:T(2,128)(2,1)} %reshape.235), calls=%async_computation.2 | async-start | bytes 655360 | tf_op jit(solution)/shard_map/all_to_all | solution.py:137
  145.3 8.4 %copy-start.17 = (f32[16]{0:T(128)S(1)}, f32[16]{0:T(128)}, u32[]{:S(2)}) copy-start(f32[16]{0:T(128)} %param.12) | copy-start | bytes 196
  145.3 8.7 %copy-start.9 = (bf16[4,2,20480]{2,1,0:T(2,128)(2,1)S(1)}, bf16[4,2,20480]{2,1,0:T(2,128)(2,1)}, u32[]{:S(2)}) copy-start(bf16[4,2,20480]{2,1,0:T(2,128)(2,1)} %copy-done.8) | copy-start | bytes 983044
  149.5 13.5 %all-to-all-start = ((bf16[4,2,40960]{2,1,0:T(2,128)(2,1)}), bf16[4,2,40960]{2,1,0:T(2,128)(2,1)S(1)}, u32[]{:S(2)}, u32[]{:S(2)}) async-start(bf16[4,2,40960]{2,1,0:T(2,128)(2,1)} %reshape.231), calls=%async_computation | async-start | bytes 1310720 | tf_op jit(solution)/shard_map/all_to_all | solution.py:135
  153.7 262.3 %reduce-scatter.2.cloned.1.call-start = ((), (), s32[]{:S(2)}) async-start(), calls=%async_computation.8 | async-start | bytes 9437184 | tf_op jit(solution)/shard_map/reduce_scatter | solution.py:170
  155.6 1.9 copy-start.11
  169.3 4.9 %copy-start.13 = (bf16[640,4,2,32]{0,3,2,1:T(8,128)(2,1)}, bf16[640,4,2,32]{0,3,2,1:T(8,128)(2,1)S(1)}, u32[]{:S(2)}) copy-start(bf16[640,4,2,32]{0,3,2,1:T(8,128)(2,1)S(1)} %get-tuple-element.384) | copy-start | bytes 983044 | tf_op jit(solution)/shard_map/while
  185.8 2.5 copy-start.2
  185.8 2.6 copy-start.3
  185.8 2.8 copy-start.4
  188.6 6.0 %copy-start.14 = (bf16[640,4,2,32]{0,3,2,1:T(8,128)(2,1)S(1)}, bf16[640,4,2,32]{0,3,2,1:T(8,128)(2,1)}, u32[]{:S(2)}) copy-start(bf16[640,4,2,32]{0,3,2,1:T(8,128)(2,1)} %copy-done.13) | copy-start | bytes 983044 | tf_op jit(solution)/shard_map/while
  189.9 4.7 copy-start.5
  194.6 4.9 %copy-start.13 = (bf16[640,4,2,32]{0,3,2,1:T(8,128)(2,1)}, bf16[640,4,2,32]{0,3,2,1:T(8,128)(2,1)S(1)}, u32[]{:S(2)}) copy-start(bf16[640,4,2,32]{0,3,2,1:T(8,128)(2,1)S(1)} %get-tuple-element.384) | copy-start | bytes 983044 | tf_op jit(solution)/shard_map/while
  212.2 2.5 copy-start.2
  212.2 2.6 copy-start.3
  212.2 2.8 copy-start.4
  214.9 6.0 %copy-start.14 = (bf16[640,4,2,32]{0,3,2,1:T(8,128)(2,1)S(1)}, bf16[640,4,2,32]{0,3,2,1:T(8,128)(2,1)}, u32[]{:S(2)}) copy-start(bf16[640,4,2,32]{0,3,2,1:T(8,128)(2,1)} %copy-done.13) | copy-start | bytes 983044 | tf_op jit(solution)/shard_map/while
  216.2 4.7 copy-start.5
  220.9 4.9 %copy-start.13 = (bf16[640,4,2,32]{0,3,2,1:T(8,128)(2,1)}, bf16[640,4,2,32]{0,3,2,1:T(8,128)(2,1)S(1)}, u32[]{:S(2)}) copy-start(bf16[640,4,2,32]{0,3,2,1:T(8,128)(2,1)S(1)} %get-tuple-element.384) | copy-start | bytes 983044 | tf_op jit(solution)/shard_map/while
  238.5 2.5 copy-start.2
  238.5 2.6 copy-start.3
  238.5 2.8 copy-start.4
  241.2 6.0 %copy-start.14 = (bf16[640,4,2,32]{0,3,2,1:T(8,128)(2,1)S(1)}, bf16[640,4,2,32]{0,3,2,1:T(8,128)(2,1)}, u32[]{:S(2)}) copy-start(bf16[640,4,2,32]{0,3,2,1:T(8,128)(2,1)} %copy-done.13) | copy-start | bytes 983044 | tf_op jit(solution)/shard_map/while
  242.6 4.7 copy-start.5
  247.2 4.9 %copy-start.13 = (bf16[640,4,2,32]{0,3,2,1:T(8,128)(2,1)}, bf16[640,4,2,32]{0,3,2,1:T(8,128)(2,1)S(1)}, u32[]{:S(2)}) copy-start(bf16[640,4,2,32]{0,3,2,1:T(8,128)(2,1)S(1)} %get-tuple-element.384) | copy-start | bytes 983044 | tf_op jit(solution)/shard_map/while
  264.8 2.5 copy-start.2
  264.8 2.6 copy-start.3
  264.8 2.8 copy-start.4
  267.6 6.0 %copy-start.14 = (bf16[640,4,2,32]{0,3,2,1:T(8,128)(2,1)S(1)}, bf16[640,4,2,32]{0,3,2,1:T(8,128)(2,1)}, u32[]{:S(2)}) copy-start(bf16[640,4,2,32]{0,3,2,1:T(8,128)(2,1)} %copy-done.13) | copy-start | bytes 983044 | tf_op jit(solution)/shard_map/while
  268.9 4.7 copy-start.5
  273.6 4.9 %copy-start.13 = (bf16[640,4,2,32]{0,3,2,1:T(8,128)(2,1)}, bf16[640,4,2,32]{0,3,2,1:T(8,128)(2,1)S(1)}, u32[]{:S(2)}) copy-start(bf16[640,4,2,32]{0,3,2,1:T(8,128)(2,1)S(1)} %get-tuple-element.384) | copy-start | bytes 983044 | tf_op jit(solution)/shard_map/while
  291.1 2.5 copy-start.2
  291.1 2.6 copy-start.3
  291.1 2.8 copy-start.4
  293.9 6.0 %copy-start.14 = (bf16[640,4,2,32]{0,3,2,1:T(8,128)(2,1)S(1)}, bf16[640,4,2,32]{0,3,2,1:T(8,128)(2,1)}, u32[]{:S(2)}) copy-start(bf16[640,4,2,32]{0,3,2,1:T(8,128)(2,1)} %copy-done.13) | copy-start | bytes 983044 | tf_op jit(solution)/shard_map/while
  295.2 4.7 copy-start.5
  299.9 1.5 copy-start.6
  333.3 84.9 %all-to-all-start.4 = ((bf16[4,2,20480]{2,1,0:T(2,128)(2,1)}), bf16[4,2,20480]{2,1,0:T(2,128)(2,1)S(1)}, u32[]{:S(2)}, u32[]{:S(2)}) async-start(bf16[4,2,20480]{2,1,0:T(2,128)(2,1)} %reshape.239), calls=%async_computation.4 | async-start | bytes 655360 | tf_op jit(solution)/shard_map/all_to_all | solution.py:159
  336.8 133.6 %all-reduce.2.cloned.1.call-start = ((), (), s32[]{:S(2)}) async-start(), calls=%async_computation.9 | async-start | bytes 2097152 | tf_op jit(solution)/shard_map/psum | solution.py:178
  420.2 3.8 copy-start.7
  (6 other events, 5.6 us)
Sparse Core Ops, SparseCore 0:
  10.2 50.5 all-gather.4
  62.9 46.0 all-gather.2
  328.0 87.8 reduce-scatter.1
  419.4 50.9 all-reduce.1
where the time goes:
time: 488 us; the launch traced here: 481 us
  waiting for transfers between devices  200 us (41%)
  matrix products  99.6 us (20%)
  local copies, waits for them, and re-layouts  84.4 us (17%)
  other arithmetic  53 us (11%)
  starting transfers between devices  17 us (3%)
  between operations  14.5 us (3%)
  blocking collectives  11.9 us (2%)
    reduce_scatter x1, waiting for transfers between devices, body(): lax.psum_scatter(lax.dot_general(token_block, packed_rows, outer_rows, pr...  79.1 us
    psum x1, waiting for transfers between devices, body(): grad_total = lax.psum(grad_shard, 'sp').astype(jnp.float32)  44.7 us
    all_gather x1, waiting for transfers between devices, body(): lax.all_gather(query_weight, 'dp', axis=0, tiled=True)  43.2 us
    dot_general x20, matrix products, pair_product(): jnp.einsum(pattern, first_op, second_op, preferred_element_type=jnp.float32)  34.7 us
    all_gather x1, waiting for transfers between devices, body(): lax.all_gather(key_weight, 'dp', axis=0, tiled=True)  31.4 us
    unnamed x7, other arithmetic  27.8 us
    unnamed x44, local copies, waits for them, and re-layouts  24 us
    dynamic_update_slice x5, local copies, waits for them, and re-layouts, head_backward(): lax.scan(block_step, zero_init, (query_split, grad_split, block_starts))  23.3 us
  transfers between devices with their start and end apart: 8, of which 5 were waited for; matrix products, arithmetic and copies ran while one was open for 16% of the time, Pallas kernels for 0%

commit v1 on v0

v1 whole, which is shorter than its diff:
```python
import functools
import math

import jax
import jax.numpy as jnp
from jax import lax
from jax.experimental import pallas as pl
from jax.experimental.pallas import tpu as pltpu
from jax.sharding import PartitionSpec as P

DQK = 32
NORM_EPS = 0.1
THETA = 10000.0
F32 = jnp.float32
BF16 = jnp.bfloat16


def dot(a, b, ca=1, cb=0):
    return lax.dot_general(a, b, (((ca,), (cb,)), ((), ())), preferred_element_type=F32)


def rotation_tables(seq_length):
    half = DQK // 2
    freqs = jnp.exp(-math.log(THETA) * jnp.arange(half, dtype=F32) / half)
    angles = freqs[:, None] * jnp.arange(seq_length, dtype=jnp.int32).astype(F32)[None, :]
    return jnp.cos(angles), jnp.sin(angles)


def rotate_rows(x, cos, sin):
    half = DQK // 2
    parts = []
    for g in range(x.shape[0] // DQK):
        a = x[g * DQK : g * DQK + half]
        b = x[g * DQK + half : (g + 1) * DQK]
        parts += [a * cos - b * sin, b * cos + a * sin]
    return jnp.concatenate(parts, axis=0)


def attention_kernel(heads, lam_ref, cos_ref, sin_ref, qk_ref, v_ref, og_ref, back_ref, dv_ref,
                     vt_s, ogt_s, dvt_s, dk_s):
    seq = cos_ref.shape[1]
    qc = qk_ref.shape[0] // 2
    hw = qc // heads
    ve = v_ref.shape[1] // heads
    inv_root = 1.0 / math.sqrt(DQK)
    vt_s[...] = v_ref[...].T
    ogt_s[...] = og_ref[...].T
    step = 256

    def one_head(h, _):
        lam = lam_ref[h]
        cos, sin = cos_ref[...], sin_ref[...]
        qrow = pl.multiple_of(h * hw, hw)
        vrow = pl.multiple_of(h * ve, ve)
        qt = rotate_rows(qk_ref[pl.ds(qrow, hw), :], cos, sin).astype(BF16)
        kt = rotate_rows(qk_ref[pl.ds(qc + qrow, hw), :], cos, sin).astype(BF16)
        k = kt.T
        vt = vt_s[pl.ds(vrow, ve), :]
        v = vt.T
        zero_half = jnp.zeros((DQK, step), BF16)
        dk_s[...] = jnp.zeros_like(dk_s)
        dvt_s[pl.ds(vrow, ve), :] = jnp.zeros((ve, seq), F32)
        for t0 in range(0, seq, step):
            end = min(t0 + step, seq)
            tb = end - t0
            zh = zero_half[:, :tb]
            q_b = qt[:, t0:end]
            mask = lax.broadcasted_iota(jnp.int32, (tb, tb), 0) <= lax.broadcasted_iota(
                jnp.int32, (tb, tb), 1
            )
            probs = []
            for m in range(2):
                half_q = q_b[m * DQK : (m + 1) * DQK]
                rhs = jnp.concatenate([half_q, zh] if m == 0 else [zh, half_q], axis=0)
                s = dot(k[:end], rhs) * inv_root
                diag = jnp.where(mask, s[t0:], -jnp.inf)
                s = jnp.concatenate([s[:t0], diag], axis=0) if t0 else diag
                e = jnp.exp(s - jnp.max(s, axis=0, keepdims=True))
                probs.append(e * (1.0 / jnp.sum(e, axis=0, keepdims=True)))
            p1, p2 = probs
            mix = (p1 - lam * p2).astype(BF16)
            ho = dot(vt[:, :end], mix)
            inv = lax.rsqrt(jnp.mean(ho * ho, axis=0, keepdims=True) + NORM_EPS)
            og = ogt_s[pl.ds(vrow, ve), t0:end].astype(F32)
            ob = (inv * og - inv * inv * inv * ho * jnp.mean(og * ho, axis=0, keepdims=True)).astype(BF16)
            mg = dot(v[:end], ob) * inv_root
            g1 = (p1 * (mg - jnp.sum(mg * p1, axis=0, keepdims=True))).astype(BF16)
            g2 = ((-lam * p2) * (mg - jnp.sum(mg * p2, axis=0, keepdims=True))).astype(BF16)
            dvt_s[pl.ds(vrow, ve), :end] += dot(ob, mix, 1, 1)
            dq = jnp.concatenate([dot(kt[:DQK, :end], g1), dot(kt[DQK:, :end], g2)], axis=0)
            back_ref[pl.ds(qrow, hw), t0:end] = rotate_rows(dq, cos[:, t0:end], -sin[:, t0:end]).astype(BF16)
            dk_s[:DQK, :end] += dot(q_b[:DQK], g1, 1, 1)
            dk_s[DQK:, :end] += dot(q_b[DQK:], g2, 1, 1)
        back_ref[pl.ds(qc + qrow, hw), :] = rotate_rows(dk_s[...], cos, -sin).astype(BF16)
        return 0

    lax.fori_loop(0, heads, one_head, 0)
    dv_ref[...] = dvt_s[...].T.astype(BF16)


def attention(qkt, v_all, og_all, lam, cos, sin):
    heads = lam.shape[0]
    seq = v_all.shape[0]
    vc = v_all.shape[1]
    vm = pl.BlockSpec(memory_space=pltpu.VMEM)
    return pl.pallas_call(
        functools.partial(attention_kernel, heads),
        out_shape=(
            jax.ShapeDtypeStruct(qkt.shape, BF16),
            jax.ShapeDtypeStruct(v_all.shape, BF16),
        ),
        in_specs=[pl.BlockSpec(memory_space=pltpu.SMEM)] + [vm] * 5,
        out_specs=(vm, vm),
        scratch_shapes=[
            pltpu.VMEM((vc, seq), BF16),
            pltpu.VMEM((vc, seq), BF16),
            pltpu.VMEM((vc, seq), F32),
            pltpu.VMEM((qkt.shape[0] // heads // 2, seq), F32),
        ],
        compiler_params=pltpu.CompilerParams(vmem_limit_bytes=60 * 1024 * 1024),
        name="attn",
    )(lam, cos, sin, qkt, v_all, og_all)


def body(tokens, query_weight, key_weight, values, lambdas, out_grad):
    sp = lax.axis_size("sp")
    dp = lax.axis_size("dp")
    rows = tokens.shape[1]
    seq = rows * sp
    heads = lambdas.shape[0] // sp
    qc = query_weight.shape[1] // sp
    me = lax.axis_index("sp")
    lam = lax.dynamic_slice_in_dim(lambdas, me * heads, heads)
    cos, sin = rotation_tables(seq)
    w_loc = jnp.concatenate(
        [lax.dynamic_slice_in_dim(w, me * qc, qc, axis=1) for w in (query_weight, key_weight)], axis=1
    )
    w_all = lax.all_gather(w_loc, "dp", axis=0, tiled=True)
    tok_all = lax.all_gather(tokens[0], "sp", axis=0, tiled=True)
    v_all = lax.all_to_all(values[0], "sp", split_axis=1, concat_axis=0, tiled=True)
    og_all = lax.all_to_all(out_grad[0], "sp", split_axis=1, concat_axis=0, tiled=True)
    qkt = dot(w_all, tok_all, 0, 1)
    back, dv = attention(qkt, v_all, og_all, lam, cos, sin)
    wgrad = dot(tok_all, back, 0, 1).astype(BF16)
    tgrad = dot(back, w_all, 0, 1).astype(BF16)
    wshard = lax.psum_scatter(wgrad, "dp", scatter_dimension=0, tiled=True)
    tokens_grad = lax.psum_scatter(tgrad, "sp", scatter_dimension=0, tiled=True)
    values_grad = lax.all_to_all(dv, "sp", split_axis=0, concat_axis=1, tiled=True)
    wfull = lax.all_gather(wshard, "sp", axis=0)
    wfull = jnp.transpose(wfull, (1, 0, 2)).astype(F32) * (1.0 / math.sqrt(dp * seq))
    n = wfull.shape[0]
    qg = wfull[:, :, :qc].reshape(n, sp * qc)
    kg = wfull[:, :, qc:].reshape(n, sp * qc)
    return tokens_grad[None], values_grad[None], qg, kg


def solution(mesh):
    x = P("dp", "sp", None)
    w = P("dp", None)
    return jax.shard_map(
        body, mesh=mesh, in_specs=(x, w, w, x, P(), x), out_specs=(x, x, w, w), check_vma=False
    )
```

time: 488 us -> 224 us (0.46); the launches traced: 481 us -> 223 us
  matrix products: 99.6 us -> 13.8 us
  local copies, waits for them, and re-layouts: 84.4 us -> 14.6 us
  waiting for transfers between devices: 200 us -> 141 us
  other arithmetic: 53 us -> 4.47 us
  Pallas kernels: 0 us -> 16.1 us
  starting transfers between devices: 17 us -> 8.85 us
    psum x1 -> x0, waiting for transfers between devices: 44.7 us -> none  [body(): grad_total = lax.psum(grad_shard, 'sp').astype(jnp.float32)]
    sub x15 -> x0, matrix products: 44.3 us -> none  [the longest x5 17 us: block_step(): exp_scores = jnp.exp(scores - row_max)]
    dot_general x25 -> x3, matrix products: 55.3 us -> 13.8 us  [dot(): lax.dot_general(a, b, (((ca,), (cb,)), ((), ())), preferred_element_type=...]
    unnamed x7 -> x0, other arithmetic: 27.8 us -> none
    dynamic_update_slice x5 -> x0, local copies, waits for them, and re-layouts: 23.3 us -> none  [head_backward(): lax.scan(block_step, zero_init, (query_split, grad_split, block_starts))]
    unnamed x44 -> x18, local copies, waits for them, and re-layouts: 24 us -> 4.02 us
    pallas_call x0 -> x1, Pallas kernels: none -> 16.1 us  [attention(): pl.pallas_call(functools.partial(attention_kernel, heads), out_shape=(jax...]
    convert_element_type x2 -> x0, local copies, waits for them, and re-layouts: 12.6 us -> none  [the longest x1 11.7 us: body(): packed = jnp.stack((query_rot, key_rot), axis=2).reshape(1, tok_rows, hea...]
  transfers between devices with their start and end apart: 8 -> 7, of which waited for: 5 -> 6; matrix products, arithmetic and copies ran while one was open for 16% -> 11% of each run, Pallas kernels for 0% -> 0%
where the time goes in v1:
time: 224 us; the launch traced here: 223 us
  waiting for transfers between devices  141 us (63%)
  Pallas kernels  16.1 us (7%)
  local copies, waits for them, and re-layouts  14.6 us (7%)
  between operations  13.9 us (6%)
  matrix products  13.8 us (6%)
  blocking collectives  10.3 us (5%)
  starting transfers between devices  8.85 us (4%)
  other arithmetic  4.47 us (2%)
    all_gather x1, waiting for transfers between devices, body(): tok_all = lax.all_gather(tokens[0], 'sp', axis=0, tiled=True)  40.8 us
    reduce_scatter x1, waiting for transfers between devices, body(): wshard = lax.psum_scatter(wgrad, 'dp', scatter_dimension=0, tiled=True)  36.2 us
    reduce_scatter x1, waiting for transfers between devices, body(): tokens_grad = lax.psum_scatter(tgrad, 'sp', scatter_dimension=0, tiled=True)  32 us
    all_gather x1, waiting for transfers between devices, body(): w_all = lax.all_gather(w_loc, 'dp', axis=0, tiled=True)  16.7 us
    pallas_call x1, Pallas kernels, attention(): pl.pallas_call(functools.partial(attention_kernel, heads), out_shape=(jax...  16.1 us
    dot_general x3, matrix products, dot(): lax.dot_general(a, b, (((ca,), (cb,)), ((), ())), preferred_element_type=...  13.8 us
    all_gather x1, waiting for transfers between devices, body(): wfull = lax.all_gather(wshard, 'sp', axis=0)  11.5 us
    all_to_all x1, blocking collectives, body(): lax.all_to_all(dv, 'sp', split_axis=0, concat_axis=1, tiled=True)  10.3 us
  transfers between devices with their start and end apart: 7, of which 6 were waited for; matrix products, arithmetic and copies ran while one was open for 11% of the time, Pallas kernels for 0%

profile of v1, /device:TPU:0, one launch (start us, length us, event | category | flops | bytes accessed | tf_op | source)
XLA Modules:
  0.0 223.4 jit_solution(18055530921885841119)
XLA Ops:
  7.2 0.0 copy-start.2
  7.2 0.0 copy-start.3
  7.2 0.0 all-gather.6.cloned.1.call-start
  7.2 1.0 constant_dynamic-slice_fusion
  8.3 0.7 pad_maximum_fusion
  9.0 0.0 all-gather.6.cloned.1.call-update
  9.0 0.0 all-gather.8.cloned.1.call-start
  9.1 0.7 all-gather.8.cloned.1.call-update
  9.8 0.0 copy-done.2
  9.8 0.2 all_to_all.40
  10.0 0.8 copy.10
  10.8 5.2 %all-to-all-start = ((bf16[160,4,256]{2,0,1:T(8,128)(2,1)}), bf16[160,4,256]{2,0,1:T(8,128)(2,1)S(1)}, u32[]{:S(2)}, u32[]{:S(2)}) async-start(bf16[160,4,256]{2,0,1:T(8,128)(2,1)} %copy.10), calls=%async_computation | async-start | bytes 655360 | tf_op jit(solution)/shard_map/all_to_all | solution.py:140
  16.0 0.0 copy-done.3
  16.0 0.2 all_to_all.44
  16.2 0.8 copy.11
  17.0 0.0 copy-done.7
  17.0 0.6 dynamic_slice.9.lam_ref
  17.6 0.9 multiply_sine_fusion
  18.5 3.4 %all-to-all-done = bf16[160,4,256]{2,0,1:T(8,128)(2,1)S(1)} async-done(((bf16[160,4,256]{2,0,1:T(8,128)(2,1)}), bf16[160,4,256]{2,0,1:T(8,128)(2,1)S(1)}, u32[]{:S(2)}, u32[]{:S(2)}) %all-to-all-start) | async-done | bytes 327712 | tf_op jit(solution)/shard_map/all_to_all | solution.py:140
  21.9 3.5 %all-to-all-start.1 = ((bf16[160,4,256]{2,0,1:T(8,128)(2,1)}), bf16[160,4,256]{2,0,1:T(8,128)(2,1)S(1)}, u32[]{:S(2)}, u32[]{:S(2)}) async-start(bf16[160,4,256]{2,0,1:T(8,128)(2,1)} %copy.11), calls=%async_computation.1 | async-start | bytes 655360 | tf_op jit(solution)/shard_map/all_to_all | solution.py:141
  25.3 0.0 reduce-scatter.5.cloned.1.call-start
  25.4 16.7 %all-gather.6.cloned.1.call-done = bf16[2048,512]{1,0:T(8,128)(2,1)} async-done(((bf16[256,512]{1,0:T(8,128)(2,1)}), bf16[2048,512]{1,0:T(8,128)(2,1)}) %all-gather.6.cloned.1.call-update) | async-done | bytes 2097168 | tf_op jit(solution)/shard_map/all_gather | solution.py:138
  42.1 40.8 %all-gather.8.cloned.1.call-done = bf16[1,640,2048]{2,1,0:T(8,128)(2,1)} async-done(((bf16[1,160,2048]{2,1,0:T(8,128)(2,1)}), bf16[1,640,2048]{2,1,0:T(8,128)(2,1)}) %all-gather.8.cloned.1.call-update) | async-done | bytes 2621456 | tf_op jit(solution)/shard_map/all_gather | solution.py:139
  82.9 5.4 %fusion.2.qk_ref = f32[512,640]{1,0:T(8,128)} fusion(bf16[2048,512]{1,0:T(8,128)(2,1)} %all-gather.6.cloned.1.call-done, bf16[1,640,2048]{2,1,0:T(8,128)(2,1)} %all-gather.8.cloned.1.call-done), kind=kOutput, calls=%fused_computation.4 | convolution fusion | flops 1342177280 | bytes 6029312 | tf_op jit(solution)/shard_map/dot_general | solution.py:19
  88.3 0.0 all-to-all-done.1
  88.3 0.7 copy-done.1
  89.0 16.1 %attn.1 = (bf16[512,640]{1,0:T(8,128)(2,1)}, bf16[640,256]{1,0:T(8,128)(2,1)}) custom-call(f32[4]{0:T(128)} %dynamic_slice.9.lam_ref, f32[16,640]{1,0:T(8,128)} %get-tuple-element.11.cos_ref, f32[16,640]{1,0:T(8,128)} %get-tuple-element.10.sin_ref, f32[512,640]{1,0:T(8,128)} %fusion.2.qk_ref, bf16[640,256]{1,0:T(8,128)(2,1)} %bitcast.30, ...), custom_call_target="tpu_custom_call" | custom-call | tf_op jit(solution)/shard_map/attn/pallas_call | solution.py:106
  105.1 4.2 %fusion = bf16[2048,512]{0,1:T(8,128)(2,1)} fusion(bf16[512,640]{1,0:T(8,128)(2,1)} %get-tuple-element.6, bf16[1,640,2048]{2,1,0:T(8,128)(2,1)S(1)} %copy-done.5), kind=kOutput, calls=%fused_computation.2 | convolution fusion | flops 1343225856 | bytes 5373952 | tf_op jit(solution)/shard_map/dot_general | solution.py:19
  109.3 0.0 reduce-scatter.5.cloned.1.call-update
  109.3 0.0 all-gather.10.cloned.1.call-start
  109.4 36.2 %reduce-scatter.5.cloned.1.call-done = bf16[256,512]{0,1:T(8,128)(2,1)} async-done(((bf16[2048,512]{0,1:T(8,128)(2,1)}), bf16[256,512]{0,1:T(8,128)(2,1)}) %reduce-scatter.5.cloned.1.call-update) | async-done | bytes 262160 | tf_op jit(solution)/shard_map/reduce_scatter | solution.py:146
  145.6 0.0 all-gather.10.cloned.1.call-update
  145.6 0.0 reduce-scatter.3.cloned.1.call-start
  145.7 4.2 %convolution_convert_fusion = bf16[640,2048]{1,0:T(8,128)(2,1)} fusion(bf16[512,640]{1,0:T(8,128)(2,1)} %get-tuple-element.6, bf16[2048,512]{1,0:T(8,128)(2,1)S(1)} %copy-done.6), kind=kOutput, calls=%fused_computation | convolution fusion | flops 1343488000 | bytes 5373952 | tf_op jit(solution)/shard_map/dot_general | solution.py:19
  149.9 0.0 reduce-scatter.3.cloned.1.call-update
  149.9 0.9 copy-done.4
  150.8 10.3 %all_to_all.54 = bf16[4,160,256]{2,1,0:T(8,128)(2,1)S(1)} all-to-all(bf16[4,160,256]{2,1,0:T(8,128)(2,1)S(1)} %bitcast.35), channel_id=1, replica_groups=mesh['sp'=4,'dp'=8] {'sp'}, dimensions={0} | all-to-all | bytes 655360 | tf_op jit(solution)/shard_map/all_to_all | solution.py:148
  161.2 0.3 copy.12
  161.4 0.9 broadcast_in_dim.9
  162.4 11.5 %all-gather.10.cloned.1.call-done = bf16[1024,512]{0,1:T(8,128)(2,1)} async-done(((bf16[256,512]{0,1:T(8,128)(2,1)}), bf16[1024,512]{0,1:T(8,128)(2,1)}) %all-gather.10.cloned.1.call-update) | async-done | bytes 1048592 | tf_op jit(solution)/shard_map/all_gather | solution.py:149
  173.9 2.9 %convert_multiply_fusion = f32[1024,512]{0,1:T(8,128)} fusion(bf16[1024,512]{0,1:T(8,128)(2,1)} %all-gather.10.cloned.1.call-done), kind=kLoop, calls=%fused_computation.6 | loop fusion | flops 1048576 | bytes 3145728 | tf_op jit(solution)/shard_map/mul | solution.py:150
  176.7 2.2 reshape.41
  178.9 1.3 fusion.4
  180.3 1.5 copy.14
  181.8 1.2 copy.16
  183.0 0.7 copy.13
  183.7 1.2 copy.15
  184.8 32.0 %reduce-scatter.3.cloned.1.call-done = bf16[160,2048]{1,0:T(8,128)(2,1)} async-done(((bf16[640,2048]{1,0:T(8,128)(2,1)}), bf16[160,2048]{1,0:T(8,128)(2,1)}) %reduce-scatter.3.cloned.1.call-update) | async-done | bytes 655376 | tf_op jit(solution)/shard_map/reduce_scatter | solution.py:147
  (11 shorter events, 0.0 us)
Async XLA Ops:
  7.2 2.6 %copy-start.2 = (bf16[1,160,1024]{2,1,0:T(8,128)(2,1)S(1)}, bf16[1,160,1024]{2,1,0:T(8,128)(2,1)}, u32[]{:S(2)}) copy-start(bf16[1,160,1024]{2,1,0:T(8,128)(2,1)} %param.9) | copy-start | bytes 983044
  7.2 8.8 %copy-start.3 = (bf16[1,160,1024]{2,1,0:T(8,128)(2,1)S(1)}, bf16[1,160,1024]{2,1,0:T(8,128)(2,1)}, u32[]{:S(2)}) copy-start(bf16[1,160,1024]{2,1,0:T(8,128)(2,1)} %param.11) | copy-start | bytes 983044
  7.2 34.9 %all-gather.6.cloned.1.call-start = ((), (), s32[]{:S(2)}) async-start(), calls=%async_computation.5 | async-start | bytes 2359296 | tf_op jit(solution)/shard_map/all_gather | solution.py:138
  9.0 8.0 %copy-start.7 = (f32[16]{0:T(128)S(1)}, f32[16]{0:T(128)}, u32[]{:S(2)}) copy-start(f32[16]{0:T(128)} %param.10) | copy-start | bytes 196
  9.0 73.8 %all-gather.8.cloned.1.call-start = ((), (), s32[]{:S(2)}) async-start(), calls=%async_computation.8 | async-start | bytes 3276800 | tf_op jit(solution)/shard_map/all_gather | solution.py:139
  10.8 11.1 %all-to-all-start = ((bf16[160,4,256]{2,0,1:T(8,128)(2,1)}), bf16[160,4,256]{2,0,1:T(8,128)(2,1)S(1)}, u32[]{:S(2)}, u32[]{:S(2)}) async-start(bf16[160,4,256]{2,0,1:T(8,128)(2,1)} %copy.10), calls=%async_computation | async-start | bytes 655360 | tf_op jit(solution)/shard_map/all_to_all | solution.py:140
  21.9 66.4 %copy-start = (bf16[160,4,256]{2,0,1:T(8,128)(2,1)}, bf16[160,4,256]{2,0,1:T(8,128)(2,1)S(1)}, u32[]{:S(2)}) copy-start(bf16[160,4,256]{2,0,1:T(8,128)(2,1)S(1)} %all-to-all-done) | copy-start | bytes 983044
  21.9 66.4 %all-to-all-start.1 = ((bf16[160,4,256]{2,0,1:T(8,128)(2,1)}), bf16[160,4,256]{2,0,1:T(8,128)(2,1)S(1)}, u32[]{:S(2)}, u32[]{:S(2)}) async-start(bf16[160,4,256]{2,0,1:T(8,128)(2,1)} %copy.11), calls=%async_computation.1 | async-start | bytes 655360 | tf_op jit(solution)/shard_map/all_to_all | solution.py:141
  25.3 120.3 %reduce-scatter.5.cloned.1.call-start = ((), (), s32[]{:S(2)}) async-start(), calls=%async_computation.7 | async-start | bytes 2359296 | tf_op jit(solution)/shard_map/reduce_scatter | solution.py:146
  82.9 22.2 %copy-start.5 = (bf16[1,640,2048]{2,1,0:T(8,128)(2,1)S(1)}, bf16[1,640,2048]{2,1,0:T(8,128)(2,1)}, u32[]{:S(2)}) copy-start(bf16[1,640,2048]{2,1,0:T(8,128)(2,1)} %all-gather.8.cloned.1.call-done) | copy-start | bytes 7864324
  88.3 0.7 copy-start.1
  109.3 36.4 %copy-start.6 = (bf16[2048,512]{1,0:T(8,128)(2,1)S(1)}, bf16[2048,512]{1,0:T(8,128)(2,1)}, u32[]{:S(2)}) copy-start(bf16[2048,512]{1,0:T(8,128)(2,1)} %all-gather.6.cloned.1.call-done) | copy-start | bytes 6291460
  109.3 64.5 %all-gather.10.cloned.1.call-start = ((), (), s32[]{:S(2)}) async-start(), calls=%async_computation.9 | async-start | bytes 1310720 | tf_op jit(solution)/shard_map/all_gather | solution.py:149
  145.6 71.2 %reduce-scatter.3.cloned.1.call-start = ((), (), s32[]{:S(2)}) async-start(), calls=%async_computation.6 | async-start | bytes 3276800 | tf_op jit(solution)/shard_map/reduce_scatter | solution.py:147
  149.9 1.0 copy-start.4
Sparse Core Ops, SparseCore 0:
  10.2 31.8 all-gather.5
  43.9 38.8 all-gather.7
  109.5 36.1 reduce-scatter.4
  147.3 26.5 all-gather.9
  177.3 39.5 reduce-scatter.2

commit v2 on v1

--- a/solution.py
+++ b/solution.py
@@ -36,15 +36,16 @@
     return jnp.concatenate(parts, axis=0)
 
 
-def attention_kernel(heads, lam_ref, cos_ref, sin_ref, qk_ref, v_ref, og_ref, back_ref, dv_ref,
-                     vt_s, ogt_s, dvt_s, dk_s):
+def attention_kernel(heads, lam_ref, cos_ref, sin_ref, qk_in, vog_ref, back_ref, rows_ref, dv_ref,
+                     qk_ref, vt_s, ogt_s, dvt_s, dk_s):
     seq = cos_ref.shape[1]
     qc = qk_ref.shape[0] // 2
     hw = qc // heads
-    ve = v_ref.shape[1] // heads
+    ve = vog_ref.shape[2] // heads
+    qk_ref[...] = qk_in[...].T
     inv_root = 1.0 / math.sqrt(DQK)
-    vt_s[...] = v_ref[...].T
-    ogt_s[...] = og_ref[...].T
+    vt_s[...] = vog_ref[0].T
+    ogt_s[...] = vog_ref[1].T
     step = 256
 
     def one_head(h, _):
@@ -96,61 +97,289 @@
 
     lax.fori_loop(0, heads, one_head, 0)
     dv_ref[...] = dvt_s[...].T.astype(BF16)
-
-
-def attention(qkt, v_all, og_all, lam, cos, sin):
+    rows_ref[...] = back_ref[...].T
+
+
+def attention(qk, vog, lam, cos, sin):
     heads = lam.shape[0]
-    seq = v_all.shape[0]
-    vc = v_all.shape[1]
+    seq, qk_cols = qk.shape
+    vc = vog.shape[2]
     vm = pl.BlockSpec(memory_space=pltpu.VMEM)
     return pl.pallas_call(
         functools.partial(attention_kernel, heads),
         out_shape=(
-            jax.ShapeDtypeStruct(qkt.shape, BF16),
-            jax.ShapeDtypeStruct(v_all.shape, BF16),
-        ),
-        in_specs=[pl.BlockSpec(memory_space=pltpu.SMEM)] + [vm] * 5,
-        out_specs=(vm, vm),
+            jax.ShapeDtypeStruct((qk_cols, seq), BF16),
+            jax.ShapeDtypeStruct((seq, qk_cols), BF16),
+            jax.ShapeDtypeStruct((seq, vc), BF16),
+        ),
+        in_specs=[pl.BlockSpec(memory_space=pltpu.SMEM)] + [vm] * 4,
+        out_specs=(vm, vm, vm),
         scratch_shapes=[
+            pltpu.VMEM((qk_cols, seq), F32),
             pltpu.VMEM((vc, seq), BF16),
             pltpu.VMEM((vc, seq), BF16),
             pltpu.VMEM((vc, seq), F32),
-            pltpu.VMEM((qkt.shape[0] // heads // 2, seq), F32),
+            pltpu.VMEM((qk_cols // heads // 2, seq), F32),
         ],
         compiler_params=pltpu.CompilerParams(vmem_limit_bytes=60 * 1024 * 1024),
         name="attn",
-    )(lam, cos, sin, qkt, v_all, og_all)
+    )(lam, cos, sin, qk, vog)
+
+
+def sender(src, dst, ssem, rsem, device):
+    return pltpu.make_async_remote_copy(
+        src_ref=src, dst_ref=dst, send_sem=ssem, recv_sem=rsem,
+        device_id=device, device_id_type=pl.DeviceIdType.MESH,
+    )
+
+
+def places(sp, dp):
+    me, mine = lax.axis_index("sp"), lax.axis_index("dp")
+    z, core = mine // 2, lax.rem(mine, 2)
+    nz = dp // 2
+    if sp == 4:
+        peers = [me + 1 - 2 * lax.rem(me, 2), lax.rem(me + 2, 4), 3 - me]
+        froms = peers
+    else:
+        peers = [lax.rem(me + d, sp) for d in range(1, sp)]
+        froms = [lax.rem(me + sp - d, sp) for d in range(1, sp)]
+    z_to = [lax.rem(z + i, nz) * 2 for i in range(1, nz)]
+    z_from = [lax.rem(z + nz - i, nz) * 2 for i in range(1, nz)]
+    return me, mine, z, core, peers, froms, z_to, z_from
+
+
+def greet(me, mine, core, peers, z_to):
+    barrier = pltpu.get_barrier_semaphore()
+    where = [(p, mine) for p in peers] + [(me, zt + core) for zt in z_to] + [(me, mine + 1 - 2 * core)]
+    for device in where:
+        pl.semaphore_signal(barrier, inc=1, device_id=device, device_id_type=pl.DeviceIdType.MESH)
+    pl.semaphore_wait(barrier, len(where))
+
+
+def gather_kernel(sp, dp, tok_ref, vog_ref, w_ref, tok_all, vog_all, w_all, qk_ref,
+                  tok_ss, tok_rs, vog_ss, vog_rs, w_ss, w_rs, sib_ss, sib_rs):
+    me, mine, z, core, peers, froms, z_to, z_from = places(sp, dp)
+    rows, wr = tok_ref.shape[0], w_ref.shape[0]
+    sib = (me, mine + 1 - 2 * core)
+    greet(me, mine, core, peers, z_to)
+
+    def trow(i, start=0, size=rows):
+        return pl.ds(pl.multiple_of(i * rows + start, 16), size)
+
+    def wrow(i):
+        return pl.ds(pl.multiple_of(i * wr, wr), wr)
+
+    sends = []
+
+    def go(copy):
+        copy.start()
+        sends.append(copy)
+        return copy
+
+    wz = [go(sender(w_ref, w_all.at[wrow(mine)], w_ss.at[i], w_rs.at[i], (me, zt + core)))
+          for i, zt in enumerate(z_to)]
+    ws = [go(sender(w_ref, w_all.at[wrow(mine)], sib_ss.at[0], sib_rs.at[0], sib))]
+    half = rows // 2
+    if sp == 4:
+        def piece(p, h, k):
+            r = trow(me, h * half, half)
+            return go(sender(tok_ref.at[pl.ds(h * half, half)], tok_all.at[r], tok_ss.at[k], tok_rs.at[k], (p, mine)))
+
+        x0, y1 = piece(peers[0], 0, 0), piece(peers[1], 1, 1)
+        x1, y0 = piece(peers[0], 1, 2), piece(peers[1], 0, 3)
+    else:
+        tk = [go(sender(tok_ref, tok_all.at[trow(me)], tok_ss.at[i], tok_rs.at[i], (p, mine)))
+              for i, p in enumerate(peers)]
+    vg = [go(sender(vog_ref.at[p], vog_all.at[:, trow(me)], vog_ss.at[i], vog_rs.at[i], (p, mine)))
+          for i, p in enumerate(peers)]
+    tok_all[trow(me), :] = tok_ref[...]
+    vog_all[:, trow(me), :] = vog_ref[me]
+    w_all[wrow(mine), :] = w_ref[...]
+    if sp == 4:
+        x0.wait_recv()
+        f0 = trow(peers[0], 0, half)
+        d0 = go(sender(tok_all.at[f0], tok_all.at[f0], tok_ss.at[4], tok_rs.at[4], (peers[1], mine)))
+        y1.wait_recv()
+        f1 = trow(peers[1], half, half)
+        d1 = go(sender(tok_all.at[f1], tok_all.at[f1], tok_ss.at[5], tok_rs.at[5], (peers[0], mine)))
+        arrivals = [[x1], [y0], [d0, d1]]
+    else:
+        arrivals = [[c] for c in tk]
+    for i, zf in enumerate(z_from):
+        wz[i].wait_recv()
+        r = wrow(zf + core)
+        ws.append(go(sender(w_all.at[r], w_all.at[r], sib_ss.at[i + 1], sib_rs.at[i + 1], sib)))
+    for c in ws:
+        c.wait_recv()
+    qk_ref[trow(me), :] = dot(tok_ref[...], w_all[...])
+    for f, copies in zip(froms, arrivals):
+        for c in copies:
+            c.wait_recv()
+        qk_ref[trow(f), :] = dot(tok_all[trow(f), :], w_all[...])
+    for c in vg:
+        c.wait_recv()
+    for c in sends:
+        c.wait_send()
+
+
+def gather(tok, vog, w, sp, dp):
+    rows, width = tok.shape
+    vm = pl.BlockSpec(memory_space=pltpu.VMEM)
+    dma = pltpu.SemaphoreType.DMA
+    nt = 6 if sp == 4 else sp - 1
+    nz = dp // 2
+    return pl.pallas_call(
+        functools.partial(gather_kernel, sp, dp),
+        out_shape=(
+            jax.ShapeDtypeStruct((rows * sp, width), BF16),
+            jax.ShapeDtypeStruct((2, rows * sp, vog.shape[3]), BF16),
+            jax.ShapeDtypeStruct((w.shape[0] * dp, w.shape[1]), BF16),
+            jax.ShapeDtypeStruct((rows * sp, w.shape[1]), F32),
+        ),
+        in_specs=[vm] * 3,
+        out_specs=(vm,) * 4,
+        scratch_shapes=[dma((nt,)), dma((nt,)), dma((sp - 1,)), dma((sp - 1,)),
+                        dma((nz - 1,)), dma((nz - 1,)), dma((nz,)), dma((nz,))],
+        compiler_params=pltpu.CompilerParams(
+            vmem_limit_bytes=60 * 1024 * 1024, collective_id=0, has_side_effects=True
+        ),
+        name="gather",
+    )(tok, vog, w)
+
+
+def scatter_kernel(sp, dp, factor, back_t, back_m, tok_all, w_all, dv, tg_out, dv_out, qg, kg,
+                   tbuf, trecv, tacc, dvr, sib_s, sib_r, wz_s, wz_r, wacc, wg_s, wg_r,
+                   t_ss, t_rs, d_ss, d_rs, s_ss, s_rs, z_ss, z_rs, g_ss, g_rs):
+    me, mine, z, core, peers, froms, z_to, z_from = places(sp, dp)
+    nz = dp // 2
+    rows, wr = tg_out.shape[0], qg.shape[0]
+    vc = dv.shape[1]
+    qc = w_all.shape[1] // 2
+    sib = (me, mine + 1 - 2 * core)
+    greet(me, mine, core, peers, z_to)
+    sends = []
+
+    def go(copy):
+        copy.start()
+        sends.append(copy)
+        return copy
+
+    def trow(i):
+        return pl.ds(pl.multiple_of(i * rows, 16), rows)
+
+    def weight_part(owner):
+        return dot(back_t[...], tok_all[:, pl.ds(pl.multiple_of(owner * wr, wr), wr)])
+
+    def token_part(p):
+        return dot(back_m[trow(p), :], w_all[...], 1, 1)
+
+    def send_tokens(i):
+        tbuf[i] = token_part(peers[i]).astype(BF16)
+        return go(sender(tbuf.at[i], trecv.at[i], t_ss.at[i], t_rs.at[i], (peers[i], mine)))
+
+    targets = z_to + [z * 2]
+    tg = [send_tokens(0)]
+    sb = []
+    for i, zt in enumerate(targets):
+        sib_s[i] = weight_part(zt + 1 - core).astype(BF16)
+        sb.append(go(sender(sib_s.at[i], sib_r.at[i], s_ss.at[i], s_rs.at[i], sib)))
+    zs = []
+    for i, zt in enumerate(targets):
+        part = weight_part(zt + core)
+        sb[i].wait_recv()
+        part = part + sib_r[i].astype(F32)
+        if i < nz - 1:
+            wz_s[i] = part.astype(BF16)
+            zs.append(go(sender(wz_s.at[i], wz_r.at[i], z_ss.at[i], z_rs.at[i], (me, zt + core))))
+        else:
+            wacc[...] = part
+    for i in range(1, sp - 1):
+        tg.append(send_tokens(i))
+    dvc = [go(sender(dv.at[trow(p)], dvr.at[me], d_ss.at[i], d_rs.at[i], (p, mine)))
+           for i, p in enumerate(peers)]
+    dvr[me] = dv[trow(me), :]
+    tacc[...] = token_part(me)
+    for i in range(nz - 1):
+        zs[i].wait_recv()
+        wacc[...] += wz_r[i].astype(F32)
+    total = wacc[...].T.astype(BF16)
+    wg_s[...] = total
+    gs = [go(sender(wg_s, wg_r.at[me], g_ss.at[i], g_rs.at[i], (p, mine))) for i, p in enumerate(peers)]
+    wg_r[me] = total
+    for i in range(sp - 1):
+        tg[i].wait_recv()
+        tacc[...] += trecv[i].astype(F32)
+    tg_out[...] = tacc[...].astype(BF16)
+    for c in dvc:
+        c.wait_recv()
+    for s in range(sp):
+        dv_out[:, s * vc : (s + 1) * vc] = dvr[s]
+    for c in gs:
+        c.wait_recv()
+    for s in range(sp):
+        qg[:, s * qc : (s + 1) * qc] = wg_r[s, :, :qc].astype(F32) * factor
+        kg[:, s * qc : (s + 1) * qc] = wg_r[s, :, qc:].astype(F32) * factor
+    for c in sends:
+        c.wait_send()
+
+
+def scatter(back_t, back_m, tok_all, w_all, dv, sp, dp):
+    seq, width = tok_all.shape
+    rows, wr = seq // sp, width // dp
+    cols = w_all.shape[1]
+    vc = dv.shape[1]
+    nz = dp // 2
+    vm = pl.BlockSpec(memory_space=pltpu.VMEM)
+    dma = pltpu.SemaphoreType.DMA
+    factor = 1.0 / math.sqrt(dp * seq)
+    return pl.pallas_call(
+        functools.partial(scatter_kernel, sp, dp, factor),
+        out_shape=(
+            jax.ShapeDtypeStruct((rows, width), BF16),
+            jax.ShapeDtypeStruct((rows, vc * sp), BF16),
+            jax.ShapeDtypeStruct((wr, cols // 2 * sp), F32),
+            jax.ShapeDtypeStruct((wr, cols // 2 * sp), F32),
+        ),
+        in_specs=[vm] * 5,
+        out_specs=(vm,) * 4,
+        scratch_shapes=[
+            pltpu.VMEM((sp - 1, rows, width), BF16),
+            pltpu.VMEM((sp - 1, rows, width), BF16),
+            pltpu.VMEM((rows, width), F32),
+            pltpu.VMEM((sp, rows, vc), BF16),
+            pltpu.VMEM((nz, cols, wr), BF16),
+            pltpu.VMEM((nz, cols, wr), BF16),
+            pltpu.VMEM((nz - 1, cols, wr), BF16),
+            pltpu.VMEM((nz - 1, cols, wr), BF16),
+            pltpu.VMEM((cols, wr), F32),
+            pltpu.VMEM((wr, cols), BF16),
+            pltpu.VMEM((sp, wr, cols), BF16),
+            dma((sp - 1,)), dma((sp - 1,)), dma((sp - 1,)), dma((sp - 1,)), dma((nz,)), dma((nz,)),
+            dma((nz - 1,)), dma((nz - 1,)), dma((sp - 1,)), dma((sp - 1,)),
+        ],
+        compiler_params=pltpu.CompilerParams(
+            vmem_limit_bytes=62 * 1024 * 1024, collective_id=1, has_side_effects=True
+        ),
+        name="scatter",
+    )(back_t, back_m, tok_all, w_all, dv)
 
 
 def body(tokens, query_weight, key_weight, values, lambdas, out_grad):
     sp = lax.axis_size("sp")
     dp = lax.axis_size("dp")
     rows = tokens.shape[1]
-    seq = rows * sp
     heads = lambdas.shape[0] // sp
     qc = query_weight.shape[1] // sp
     me = lax.axis_index("sp")
     lam = lax.dynamic_slice_in_dim(lambdas, me * heads, heads)
-    cos, sin = rotation_tables(seq)
+    cos, sin = rotation_tables(rows * sp)
     w_loc = jnp.concatenate(
         [lax.dynamic_slice_in_dim(w, me * qc, qc, axis=1) for w in (query_weight, key_weight)], axis=1
     )
-    w_all = lax.all_gather(w_loc, "dp", axis=0, tiled=True)
-    tok_all = lax.all_gather(tokens[0], "sp", axis=0, tiled=True)
-    v_all = lax.all_to_all(values[0], "sp", split_axis=1, concat_axis=0, tiled=True)
-    og_all = lax.all_to_all(out_grad[0], "sp", split_axis=1, concat_axis=0, tiled=True)
-    qkt = dot(w_all, tok_all, 0, 1)
-    back, dv = attention(qkt, v_all, og_all, lam, cos, sin)
-    wgrad = dot(tok_all, back, 0, 1).astype(BF16)
-    tgrad = dot(back, w_all, 0, 1).astype(BF16)
-    wshard = lax.psum_scatter(wgrad, "dp", scatter_dimension=0, tiled=True)
-    tokens_grad = lax.psum_scatter(tgrad, "sp", scatter_dimension=0, tiled=True)
-    values_grad = lax.all_to_all(dv, "sp", split_axis=0, concat_axis=1, tiled=True)
-    wfull = lax.all_gather(wshard, "sp", axis=0)
-    wfull = jnp.transpose(wfull, (1, 0, 2)).astype(F32) * (1.0 / math.sqrt(dp * seq))
-    n = wfull.shape[0]
-    qg = wfull[:, :, :qc].reshape(n, sp * qc)
-    kg = wfull[:, :, qc:].reshape(n, sp * qc)
+    vog = jnp.stack([values[0], out_grad[0]]).reshape(2, rows, sp, -1).transpose(2, 0, 1, 3)
+    tok_all, vog_all, w_all, qk = gather(tokens[0], vog, w_loc, sp, dp)
+    back_t, back_m, dv = attention(qk, vog_all, lam, cos, sin)
+    tokens_grad, values_grad, qg, kg = scatter(back_t, back_m, tok_all, w_all, dv, sp, dp)
     return tokens_grad[None], values_grad[None], qg, kg
 
 

time: 224 us -> 128 us (0.57)
  waiting for transfers between devices: 141 us -> 0 us
  Pallas kernels: 16.1 us -> 114 us
  matrix products: 13.8 us -> 0 us
  between operations: 13.9 us -> 0.67 us
  blocking collectives: 10.3 us -> 0 us
  starting transfers between devices: 8.85 us -> 0 us
  local copies, waits for them, and re-layouts: 14.6 us -> 10.2 us
    pallas_call x0 -> x2, Pallas kernels: none -> 97.7 us  [the longest x1 57.6 us: scatter(): pl.pallas_call(functools.partial(scatter_kernel, sp, dp, factor), out_sha...]
    all_gather x3 -> x0, waiting for transfers between devices: 68.9 us -> none  [the longest x1 40.8 us: body(): tok_all = lax.all_gather(tokens[0], 'sp', axis=0, tiled=True)]
    reduce_scatter x2 -> x0, waiting for transfers between devices: 68.2 us -> none  [the longest x1 36.2 us: body(): wshard = lax.psum_scatter(wgrad, 'dp', scatter_dimension=0, tiled=True)]
    dot_general x3 -> x0, matrix products: 13.8 us -> none  [dot(): lax.dot_general(a, b, (((ca,), (cb,)), ((), ())), preferred_element_type=...]
    all_to_all x1 -> x0, blocking collectives: 10.3 us -> none  [body(): lax.all_to_all(dv, 'sp', split_axis=0, concat_axis=1, tiled=True)]
    all_to_all x2 -> x0, starting transfers between devices: 8.65 us -> none  [the longest x1 5.19 us: body(): lax.all_to_all(values[0], 'sp', split_axis=1, concat_axis=0, tiled=True)]
    slice x3 -> x0, local copies, waits for them, and re-layouts: 3.56 us -> none  [the longest x2 2.87 us: body(): kg = wfull[:, :, qc:].reshape(n, sp * qc)]
    all_to_all x2 -> x0, waiting for transfers between devices: 3.4 us -> none  [the longest x1 3.4 us: body(): lax.all_to_all(values[0], 'sp', split_axis=1, concat_axis=0, tiled=True)]
  transfers between devices with their start and end apart: 7 -> 0, of which waited for: 6 -> 0; matrix products, arithmetic and copies ran while one was open for 11% -> 0% of each run, Pallas kernels for 0% -> 0%
where the time goes in v2:
time: 128 us
  Pallas kernels  114 us (89%)
  local copies, waits for them, and re-layouts  10.2 us (8%)
  other arithmetic  2.73 us (2%)
    pallas_call x1, Pallas kernels, scatter(): pl.pallas_call(functools.partial(scatter_kernel, sp, dp, factor), out_sha...  57.6 us
    pallas_call x1, Pallas kernels, gather(): pl.pallas_call(functools.partial(gather_kernel, sp, dp), out_shape=(jax.S...  40 us
    pallas_call x1, Pallas kernels, attention(): pl.pallas_call(functools.partial(attention_kernel, heads), out_shape=(jax...  16.8 us
    unnamed x6, local copies, waits for them, and re-layouts  7.07 us

profile of v2, /device:TPU:0, one launch (start us, length us, event | category | flops | bytes accessed | tf_op | source)
XLA Modules:
  0.0 128.0 jit_solution(954674391122429056)
XLA Ops:
  0.6 1.2 dynamic_slice.9.lam_ref
  1.9 0.9 multiply_sine_fusion
  2.8 1.0 constant_dynamic-slice_fusion
  3.7 0.7 pad_maximum_fusion.1.w_ref
  4.5 1.1 pad_maximum_fusion
  5.6 0.9 copy.13
  6.5 40.0 %gather.1 = (bf16[640,2048]{1,0:T(8,128)(2,1)}, bf16[2,640,256]{2,1,0:T(8,128)(2,1)}, bf16[2048,512]{1,0:T(8,128)(2,1)}, f32[640,512]{1,0:T(8,128)}) custom-call(bf16[160,2048]{1,0:T(8,128)(2,1)} %bitcast.12, bf16[4,2,160,256]{3,2,1,0:T(8,128)(2,1)} %bitcast.10, bf16[256,512]{1,0:T(8,128)(2,1)} %pad_maximum_fusion.1.w_ref), custom_call_target="tpu_custom_call" | custom-call | tf_op jit(solution)/shard_map/gather/pallas_call | solution.py:231
  46.5 16.8 %attn.1 = (bf16[512,640]{1,0:T(8,128)(2,1)}, bf16[640,512]{1,0:T(8,128)(2,1)}, bf16[640,256]{1,0:T(8,128)(2,1)}) custom-call(f32[4]{0:T(128)} %dynamic_slice.9.lam_ref, f32[16,640]{1,0:T(8,128)} %get-tuple-element.27.cos_ref, f32[16,640]{1,0:T(8,128)} %get-tuple-element.26.sin_ref, f32[640,512]{1,0:T(8,128)} %get-tuple-element.15.qk_in, ...), custom_call_target="tpu_custom_call" | custom-call | tf_op jit(solution)/shard_map/attn/pallas_call | solution.py:108
  63.3 57.6 %scatter.1 = (bf16[160,2048]{1,0:T(8,128)(2,1)}, bf16[160,1024]{1,0:T(8,128)(2,1)}, f32[256,1024]{1,0:T(8,128)}, f32[256,1024]{1,0:T(8,128)}) custom-call(bf16[512,640]{1,0:T(8,128)(2,1)} %get-tuple-element.17.back_t, bf16[640,512]{1,0:T(8,128)(2,1)} %get-tuple-element.18.back_m, bf16[640,2048]{1,0:T(8,128)(2,1)} %get-tuple-element.19.tok_all, ...), custom_call_target="tpu_custom_call" | custom-call | tf_op jit(solution)/shard_map/scatter/pallas_call | solution.py:335
  120.9 0.0 copy-start
  120.9 2.1 %copy.18 = bf16[1,160,2048]{2,1,0:T(8,128)(2,1)} copy(bf16[1,160,2048]{2,1,0:T(8,128)(2,1)} %bitcast.13) | data formatting | bytes 1310720
  123.0 1.7 %copy.19 = bf16[1,160,1024]{2,1,0:T(8,128)(2,1)} copy(bf16[1,160,1024]{2,1,0:T(8,128)(2,1)} %bitcast.14) | data formatting | bytes 655360
  124.7 2.3 %copy.20 = f32[256,1024]{1,0:T(8,128)} copy(f32[256,1024]{1,0:T(8,128)} %get-tuple-element.36) | data formatting | bytes 2097152
  127.0 0.0 copy-done
  127.0 1.0 copy.21
  (2 shorter events, 0.0 us)
Async XLA Ops:
  120.9 6.1 %copy-start = (f32[256,1024]{1,0:T(8,128)S(1)}, f32[256,1024]{1,0:T(8,128)}, u32[]{:S(2)}) copy-start(f32[256,1024]{1,0:T(8,128)} %get-tuple-element.37) | copy-start | bytes 3145732

commit v3 on v2

--- a/solution.py
+++ b/solution.py
@@ -49,7 +49,7 @@
     step = 256
 
     def one_head(h, _):
-        lam = lam_ref[h]
+        lam = lam_ref[lax.axis_index("sp") * heads + h]
         cos, sin = cos_ref[...], sin_ref[...]
         qrow = pl.multiple_of(h * hw, hw)
         vrow = pl.multiple_of(h * ve, ve)
@@ -100,8 +100,7 @@
     rows_ref[...] = back_ref[...].T
 
 
-def attention(qk, vog, lam, cos, sin):
-    heads = lam.shape[0]
+def attention(qk, vog, lam, cos, sin, heads):
     seq, qk_cols = qk.shape
     vc = vog.shape[2]
     vm = pl.BlockSpec(memory_space=pltpu.VMEM)
@@ -156,12 +155,11 @@
     pl.semaphore_wait(barrier, len(where))
 
 
-def gather_kernel(sp, dp, tok_ref, vog_ref, w_ref, tok_all, vog_all, w_all, qk_ref,
-                  tok_ss, tok_rs, vog_ss, vog_rs, w_ss, w_rs, sib_ss, sib_rs):
+def gather_kernel(sp, dp, tok_ref, v_ref, og_ref, wq_ref, wk_ref, tok_all, vog_all, w_all, qk_ref,
+                  vog_ref, tok_ss, tok_rs, vog_ss, vog_rs, w_ss, w_rs, sib_ss, sib_rs):
     me, mine, z, core, peers, froms, z_to, z_from = places(sp, dp)
-    rows, wr = tok_ref.shape[0], w_ref.shape[0]
+    rows, wr = tok_ref.shape[0], wq_ref.shape[0]
     sib = (me, mine + 1 - 2 * core)
-    greet(me, mine, core, peers, z_to)
 
     def trow(i, start=0, size=rows):
         return pl.ds(pl.multiple_of(i * rows + start, 16), size)
@@ -169,6 +167,19 @@
     def wrow(i):
         return pl.ds(pl.multiple_of(i * wr, wr), wr)
 
+    vc, qc = v_ref.shape[1] // sp, wq_ref.shape[1] // sp
+    for s in range(sp):
+        vog_ref[s, 0] = v_ref[:, s * vc : (s + 1) * vc]
+        vog_ref[s, 1] = og_ref[:, s * vc : (s + 1) * vc]
+
+        @pl.when(me == s)
+        def _():
+            w_all[wrow(mine), :qc] = wq_ref[:, s * qc : (s + 1) * qc]
+            w_all[wrow(mine), qc:] = wk_ref[:, s * qc : (s + 1) * qc]
+
+    tok_all[trow(me), :] = tok_ref[...]
+    greet(me, mine, core, peers, z_to)
+    w_ref = w_all.at[wrow(mine)]
     sends = []
 
     def go(copy):
@@ -192,9 +203,7 @@
               for i, p in enumerate(peers)]
     vg = [go(sender(vog_ref.at[p], vog_all.at[:, trow(me)], vog_ss.at[i], vog_rs.at[i], (p, mine)))
           for i, p in enumerate(peers)]
-    tok_all[trow(me), :] = tok_ref[...]
     vog_all[:, trow(me), :] = vog_ref[me]
-    w_all[wrow(mine), :] = w_ref[...]
     if sp == 4:
         x0.wait_recv()
         f0 = trow(peers[0], 0, half)
@@ -222,8 +231,9 @@
         c.wait_send()
 
 
-def gather(tok, vog, w, sp, dp):
+def gather(tok, v, og, wq, wk, sp, dp):
     rows, width = tok.shape
+    vc, wr, cols = v.shape[1] // sp, wq.shape[0], 2 * wq.shape[1] // sp
     vm = pl.BlockSpec(memory_space=pltpu.VMEM)
     dma = pltpu.SemaphoreType.DMA
     nt = 6 if sp == 4 else sp - 1
@@ -232,22 +242,22 @@
         functools.partial(gather_kernel, sp, dp),
         out_shape=(
             jax.ShapeDtypeStruct((rows * sp, width), BF16),
-            jax.ShapeDtypeStruct((2, rows * sp, vog.shape[3]), BF16),
-            jax.ShapeDtypeStruct((w.shape[0] * dp, w.shape[1]), BF16),
-            jax.ShapeDtypeStruct((rows * sp, w.shape[1]), F32),
+            jax.ShapeDtypeStruct((2, rows * sp, vc), BF16),
+            jax.ShapeDtypeStruct((wr * dp, cols), BF16),
+            jax.ShapeDtypeStruct((rows * sp, cols), F32),
         ),
-        in_specs=[vm] * 3,
+        in_specs=[vm] * 5,
         out_specs=(vm,) * 4,
-        scratch_shapes=[dma((nt,)), dma((nt,)), dma((sp - 1,)), dma((sp - 1,)),
+        scratch_shapes=[pltpu.VMEM((sp, 2, rows, vc), BF16), dma((nt,)), dma((nt,)), dma((sp - 1,)), dma((sp - 1,)),
                         dma((nz - 1,)), dma((nz - 1,)), dma((nz,)), dma((nz,))],
         compiler_params=pltpu.CompilerParams(
             vmem_limit_bytes=60 * 1024 * 1024, collective_id=0, has_side_effects=True
         ),
         name="gather",
-    )(tok, vog, w)
-
-
-def scatter_kernel(sp, dp, factor, back_t, back_m, tok_all, w_all, dv, tg_out, dv_out, qg, kg,
+    )(tok, v, og, wq, wk)
+
+
+def scatter_kernel(sp, dp, back_t, back_m, tok_all, w_all, dv, tg_out, dv_out, qg, kg,
                    tbuf, trecv, tacc, dvr, sib_s, sib_r, wz_s, wz_r, wacc, wg_s, wg_r,
                    t_ss, t_rs, d_ss, d_rs, s_ss, s_rs, z_ss, z_rs, g_ss, g_rs):
     me, mine, z, core, peers, froms, z_to, z_from = places(sp, dp)
@@ -278,7 +288,18 @@
         return go(sender(tbuf.at[i], trecv.at[i], t_ss.at[i], t_rs.at[i], (peers[i], mine)))
 
     targets = z_to + [z * 2]
-    tg = [send_tokens(0)]
+    half = rows // 2
+    lo, hi = pl.ds(0, half), pl.ds(half, half)
+    tg = []
+
+    def hop(i, dst, part, k, to):
+        return go(sender(tbuf.at[i, part], trecv.at[dst, part], t_ss.at[k], t_rs.at[k], (peers[to], mine)))
+
+    if sp == 4:
+        tbuf[2] = token_part(peers[2]).astype(BF16)
+        via_x, via_y = hop(2, 2, lo, 0, 0), hop(2, 2, hi, 1, 1)
+    else:
+        tg.append(send_tokens(0))
     sb = []
     for i, zt in enumerate(targets):
         sib_s[i] = weight_part(zt + 1 - core).astype(BF16)
@@ -293,8 +314,25 @@
             zs.append(go(sender(wz_s.at[i], wz_r.at[i], z_ss.at[i], z_rs.at[i], (me, zt + core))))
         else:
             wacc[...] = part
-    for i in range(1, sp - 1):
-        tg.append(send_tokens(i))
+    if sp == 4:
+        part = token_part(peers[0])
+        tbuf[0, lo] = part[:half].astype(BF16)
+        x_lo = hop(0, 0, lo, 2, 0)
+        tacc[hi] = part[half:]
+        part = token_part(peers[1])
+        tbuf[1, hi] = part[half:].astype(BF16)
+        y_hi = hop(1, 1, hi, 3, 1)
+        tacc[lo] = part[:half]
+        via_x.wait_recv()
+        tbuf[1, lo] = (tacc[lo] + trecv[2, lo].astype(F32)).astype(BF16)
+        y_lo = hop(1, 1, lo, 4, 1)
+        via_y.wait_recv()
+        tbuf[0, hi] = (tacc[hi] + trecv[2, hi].astype(F32)).astype(BF16)
+        x_hi = hop(0, 0, hi, 5, 0)
+        tg = [x_lo, x_hi, y_lo, y_hi]
+    else:
+        for i in range(1, sp - 1):
+            tg.append(send_tokens(i))
     dvc = [go(sender(dv.at[trow(p)], dvr.at[me], d_ss.at[i], d_rs.at[i], (p, mine)))
            for i, p in enumerate(peers)]
     dvr[me] = dv[trow(me), :]
@@ -304,10 +342,29 @@
         wacc[...] += wz_r[i].astype(F32)
     total = wacc[...].T.astype(BF16)
     wg_s[...] = total
-    gs = [go(sender(wg_s, wg_r.at[me], g_ss.at[i], g_rs.at[i], (p, mine))) for i, p in enumerate(peers)]
     wg_r[me] = total
-    for i in range(sp - 1):
-        tg[i].wait_recv()
+    wh = wr // 2
+    if sp == 4:
+        def piece(p, h, k):
+            r = pl.ds(h * wh, wh)
+            return go(sender(wg_s.at[r], wg_r.at[me, r], g_ss.at[k], g_rs.at[k], (p, mine)))
+
+        def forward(f, h, k, p):
+            r = pl.ds(h * wh, wh)
+            return go(sender(wg_r.at[f, r], wg_r.at[f, r], g_ss.at[k], g_rs.at[k], (p, mine)))
+
+        gx0, gy1 = piece(peers[0], 0, 0), piece(peers[1], 1, 1)
+        gx1, gy0 = piece(peers[0], 1, 2), piece(peers[1], 0, 3)
+        gx0.wait_recv()
+        gd0 = forward(peers[0], 0, 4, peers[1])
+        gy1.wait_recv()
+        gd1 = forward(peers[1], 1, 5, peers[0])
+        gs = [gx1, gy0, gd0, gd1]
+    else:
+        gs = [go(sender(wg_s, wg_r.at[me], g_ss.at[i], g_rs.at[i], (p, mine))) for i, p in enumerate(peers)]
+    for c in tg:
+        c.wait_recv()
+    for i in range(2 if sp == 4 else sp - 1):
         tacc[...] += trecv[i].astype(F32)
     tg_out[...] = tacc[...].astype(BF16)
     for c in dvc:
@@ -317,8 +374,8 @@
     for c in gs:
         c.wait_recv()
     for s in range(sp):
-        qg[:, s * qc : (s + 1) * qc] = wg_r[s, :, :qc].astype(F32) * factor
-        kg[:, s * qc : (s + 1) * qc] = wg_r[s, :, qc:].astype(F32) * factor
+        qg[:, s * qc : (s + 1) * qc] = wg_r[s, :, :qc]
+        kg[:, s * qc : (s + 1) * qc] = wg_r[s, :, qc:]
     for c in sends:
         c.wait_send()
 
@@ -331,14 +388,14 @@
     nz = dp // 2
     vm = pl.BlockSpec(memory_space=pltpu.VMEM)
     dma = pltpu.SemaphoreType.DMA
-    factor = 1.0 / math.sqrt(dp * seq)
+    nt = 6 if sp == 4 else sp - 1
     return pl.pallas_call(
-        functools.partial(scatter_kernel, sp, dp, factor),
+        functools.partial(scatter_kernel, sp, dp),
         out_shape=(
             jax.ShapeDtypeStruct((rows, width), BF16),
             jax.ShapeDtypeStruct((rows, vc * sp), BF16),
-            jax.ShapeDtypeStruct((wr, cols // 2 * sp), F32),
-            jax.ShapeDtypeStruct((wr, cols // 2 * sp), F32),
+            jax.ShapeDtypeStruct((wr, cols // 2 * sp), BF16),
+            jax.ShapeDtypeStruct((wr, cols // 2 * sp), BF16),
         ),
         in_specs=[vm] * 5,
         out_specs=(vm,) * 4,
@@ -354,8 +411,8 @@
             pltpu.VMEM((cols, wr), F32),
             pltpu.VMEM((wr, cols), BF16),
             pltpu.VMEM((sp, wr, cols), BF16),
-            dma((sp - 1,)), dma((sp - 1,)), dma((sp - 1,)), dma((sp - 1,)), dma((nz,)), dma((nz,)),
-            dma((nz - 1,)), dma((nz - 1,)), dma((sp - 1,)), dma((sp - 1,)),
+            dma((nt,)), dma((nt,)), dma((sp - 1,)), dma((sp - 1,)), dma((nz,)), dma((nz,)),
+            dma((nz - 1,)), dma((nz - 1,)), dma((nt,)), dma((nt,)),
         ],
         compiler_params=pltpu.CompilerParams(
             vmem_limit_bytes=62 * 1024 * 1024, collective_id=1, has_side_effects=True
@@ -369,18 +426,14 @@
     dp = lax.axis_size("dp")
     rows = tokens.shape[1]
     heads = lambdas.shape[0] // sp
-    qc = query_weight.shape[1] // sp
-    me = lax.axis_index("sp")
-    lam = lax.dynamic_slice_in_dim(lambdas, me * heads, heads)
     cos, sin = rotation_tables(rows * sp)
-    w_loc = jnp.concatenate(
-        [lax.dynamic_slice_in_dim(w, me * qc, qc, axis=1) for w in (query_weight, key_weight)], axis=1
+    tok_all, vog_all, w_all, qk = gather(
+        tokens[0], values[0], out_grad[0], query_weight, key_weight, sp, dp
     )
-    vog = jnp.stack([values[0], out_grad[0]]).reshape(2, rows, sp, -1).transpose(2, 0, 1, 3)
-    tok_all, vog_all, w_all, qk = gather(tokens[0], vog, w_loc, sp, dp)
-    back_t, back_m, dv = attention(qk, vog_all, lam, cos, sin)
+    back_t, back_m, dv = attention(qk, vog_all, lambdas, cos, sin, heads)
     tokens_grad, values_grad, qg, kg = scatter(back_t, back_m, tok_all, w_all, dv, sp, dp)
-    return tokens_grad[None], values_grad[None], qg, kg
+    factor = 1.0 / math.sqrt(dp * rows * sp)
+    return tokens_grad[None], values_grad[None], qg.astype(F32) * factor, kg.astype(F32) * factor
 
 
 def solution(mesh):

time: 128 us -> 107 us (0.84); the launches traced: 128 us -> 105 us
  Pallas kernels: 114 us -> 98.6 us
  local copies, waits for them, and re-layouts: 10.2 us -> 1.57 us
    pallas_call x1, Pallas kernels: 57.6 us -> 41.4 us  [scatter(): pl.pallas_call(functools.partial(scatter_kernel, sp, dp), out_shape=(jax....]
    unnamed x6, local copies, waits for them, and re-layouts: 7.07 us -> 1.57 us
    mul x0 -> x1, other arithmetic: none -> 2.88 us  [body(): kg.astype(F32) * factor]
    dynamic_slice x2 -> x0, local copies, waits for them, and re-layouts: 2.23 us -> none  [the longest x1 1.24 us: body(): lam = lax.dynamic_slice_in_dim(lambdas, me * heads, heads)]
where the time goes in v3:
time: 107 us; the launch traced here: 105 us
  Pallas kernels  98.6 us (92%)
  other arithmetic  3.75 us (4%)
  local copies, waits for them, and re-layouts  1.57 us (1%)
    pallas_call x1, Pallas kernels, scatter(): pl.pallas_call(functools.partial(scatter_kernel, sp, dp), out_shape=(jax....  41.4 us
    pallas_call x1, Pallas kernels, gather(): pl.pallas_call(functools.partial(gather_kernel, sp, dp), out_shape=(jax.S...  40.5 us
    pallas_call x1, Pallas kernels, attention(): pl.pallas_call(functools.partial(attention_kernel, heads), out_shape=(jax...  16.8 us
    mul x1, other arithmetic, body(): kg.astype(F32) * factor  2.88 us

profile of v3, /device:TPU:0, one launch (start us, length us, event | category | flops | bytes accessed | tf_op | source)
XLA Modules:
  0.0 104.6 jit_solution(10232858303163860588)
XLA Ops:
  0.7 0.9 multiply_sine_fusion
  1.5 40.5 %gather.1 = (bf16[640,2048]{1,0:T(8,128)(2,1)}, bf16[2,640,256]{2,1,0:T(8,128)(2,1)}, bf16[2048,512]{1,0:T(8,128)(2,1)}, f32[640,512]{1,0:T(8,128)}) custom-call(bf16[160,2048]{1,0:T(8,128)(2,1)} %bitcast.5, bf16[160,1024]{1,0:T(8,128)(2,1)} %bitcast.7, bf16[160,1024]{1,0:T(8,128)(2,1)} %bitcast.8, bf16[256,1024]{1,0:T(8,128)(2,1)} %wq_ref.1, ...), custom_call_target="tpu_custom_call" | custom-call | tf_op jit(solution)/shard_map/gather/pallas_call | solution.py:241
  42.0 16.8 %attn.1 = (bf16[512,640]{1,0:T(8,128)(2,1)}, bf16[640,512]{1,0:T(8,128)(2,1)}, bf16[640,256]{1,0:T(8,128)(2,1)}) custom-call(f32[16]{0:T(128)} %lam_ref.1, f32[16,640]{1,0:T(8,128)} %get-tuple-element.27.cos_ref, f32[16,640]{1,0:T(8,128)} %get-tuple-element.26.sin_ref, f32[640,512]{1,0:T(8,128)} %get-tuple-element.15.qk_in, ...), custom_call_target="tpu_custom_call" | custom-call | tf_op jit(solution)/shard_map/attn/pallas_call | solution.py:107
  58.8 41.4 %scatter.1 = (bf16[160,2048]{1,0:T(8,128)(2,1)}, bf16[160,1024]{1,0:T(8,128)(2,1)}, bf16[256,1024]{1,0:T(8,128)(2,1)}, bf16[256,1024]{1,0:T(8,128)(2,1)}) custom-call(bf16[512,640]{1,0:T(8,128)(2,1)} %get-tuple-element.17.back_t, bf16[640,512]{1,0:T(8,128)(2,1)} %get-tuple-element.18.back_m, bf16[640,2048]{1,0:T(8,128)(2,1)} %get-tuple-element.19.tok_all, ...), custom_call_target="tpu_custom_call" | custom-call | tf_op jit(solution)/shard_map/scatter/pallas_call | solution.py:392
  100.2 0.0 copy-start
  100.2 0.0 copy-start.1
  100.2 2.9 %convert_multiply_fusion = (f32[256,1024]{1,0:T(8,128)}, f32[256,1024]{1,0:T(8,128)}) fusion(bf16[256,1024]{1,0:T(8,128)(2,1)} %get-tuple-element.25, bf16[256,1024]{1,0:T(8,128)(2,1)} %get-tuple-element.24), kind=kLoop, calls=%fused_computation | loop fusion | flops 1048576 | bytes 3145728 | tf_op jit(solution)/shard_map/mul | solution.py:436
  103.1 0.0 copy-done
  103.1 0.8 copy.12
  103.9 0.0 copy-done.1
  103.9 0.7 copy.13
  (2 shorter events, 0.0 us)
Async XLA Ops:
  100.2 2.9 %copy-start = (bf16[160,2048]{1,0:T(8,128)(2,1)S(1)}, bf16[160,2048]{1,0:T(8,128)(2,1)}, u32[]{:S(2)}) copy-start(bf16[160,2048]{1,0:T(8,128)(2,1)} %get-tuple-element.22) | copy-start | bytes 1966084
  100.2 3.7 %copy-start.1 = (bf16[160,1024]{1,0:T(8,128)(2,1)S(1)}, bf16[160,1024]{1,0:T(8,128)(2,1)}, u32[]{:S(2)}) copy-start(bf16[160,1024]{1,0:T(8,128)(2,1)} %get-tuple-element.23) | copy-start | bytes 983044
